TPU v7x, 256 devices: a whole 4x4x8 slice. The times are simulated.
256 devices in a mesh: sp: 64 (over z, y, core), tp: 4 (over x).
Axes of the slice: x: 4, y: 4, z: 8, core: 2. Of those that a mesh axis runs over, the one named last changes fastest.
Arguments:
- stream_in: bfloat16 [49152, 2048], P(('sp', 'tp')), may hold values from -6 to 6
- query_wide: bfloat16 [49152, 512], P('sp', 'tp'), may hold values from -6 to 6
- key_wide: bfloat16 [49152, 512], P('sp', 'tp'), may hold values from -6 to 6
- value_wide: bfloat16 [49152, 512], P('sp', 'tp'), may hold values from -6 to 6
- gate_wide: bfloat16 [49152, 512], P('sp', 'tp'), may hold values from -6 to 6
- decay_wide: float32 [4, 49152], P('tp', 'sp'), may hold values from -2.3 to 0, as said below
- query_narrow: bfloat16 [49152, 512], P('sp', 'tp'), may hold values from -6 to 6
- key_narrow: bfloat16 [49152, 512], P('sp', 'tp'), may hold values from -6 to 6
- value_narrow: bfloat16 [49152, 512], P('sp', 'tp'), may hold values from -6 to 6
- gate_narrow: bfloat16 [49152, 512], P('sp', 'tp'), may hold values from -6 to 6
- decay_narrow: float32 [8, 49152], P('tp', 'sp'), may hold values from -2.3 to 0, as said below
- output_wide: bfloat16 [512, 2048], P('tp'), may hold values from -0.25 to 0.25
- output_narrow: bfloat16 [512, 2048], P('tp'), may hold values from -0.25 to 0.25
- norm_gain: bfloat16 [2048], replicated, may hold values from 0.099609375 to 1.8984375
- up_weight: bfloat16 [2048, 8192], P('sp', 'tp'), may hold values from -0.125 to 0.125
- down_weight: bfloat16 [8192, 2048], P('tp', 'sp'), may hold values from -0.0625 to 0.0625
Outputs:
- layer_out: bfloat16 [49152, 2048], P(('sp', 'tp'))
Inputs may be any that keep to these rules, and one draw needn't show every extreme that they name: `decay_wide`: each entry is the logarithm of one head's retention factor at one position. `decay_narrow`: each entry is the logarithm of one head's retention factor at one position.
All inputs are finite; a program needn't handle non-finite values.
Results may differ from a plain program's by a relative error of at most 0.02.
Values may be sent and summed in bfloat16 or wider, within the bound.
A program may use at most 128 MiB of HBM per device.

v0:
```python
import jax
import jax.numpy as jnp
from jax import lax
from jax.sharding import Mesh
from jax.sharding import PartitionSpec as P

HDW = 128
HDN = 64
BLOCK = 128
SP = ("sp_0", "sp_1", "sp_2")
SP_TP = ("sp_0", "sp_1", "sp_2", "tp")
head_eps = 1e-05
norm_eps = 1e-06
rope_base = 10000.0


def rows_first(arrays, axis, dims):
    turned = [jnp.moveaxis(a, dim, 0) for a, dim in zip(arrays, dims)]
    both = jnp.concatenate([t.reshape(len(t), -1) for t in turned], axis=1)
    out, at, finished = (lax.all_gather(both, axis, axis=0, tiled=True), 0, [])
    for t, dim in zip(turned, dims):
        section = out[:, at : at + t[0].size].reshape(-1, *t.shape[1:])
        finished.append(jnp.moveaxis(section, 0, dim))
        at += t[0].size
    return tuple(finished)


def nothing_yet(shard, identity):
    return jax.tree.map(
        lambda part, zero: jnp.zeros_like(part) + jnp.asarray(zero, part.dtype), shard, identity
    )


def gathered_once(shard, axis):
    leaves = jax.tree.leaves(shard)
    sequence = sorted(range(len(leaves)), key=lambda k: -leaves[k].size)
    width = (1, *leaves[sequence[0]].shape)[-1]
    lines = [
        jnp.pad(leaves[k].reshape(-1), (0, -leaves[k].size % width)).reshape(-1, width)
        for k in sequence
    ]
    both, at, found = (lax.all_gather(jnp.concatenate(lines), axis), 0, {})
    for k, line in zip(sequence, lines):
        section = both[:, at : at + len(line)].reshape(len(both), -1)
        found[k] = section[:, : leaves[k].size].reshape(-1, *leaves[k].shape)
        at += len(line)
    numbers = iter(range(len(leaves)))
    return jax.tree.map(lambda _: found[next(numbers)], shard)


def entering(shard, axes, combine, identity):
    before = start = nothing_yet(shard, identity)
    so_far = shard
    for axis in reversed(axes):
        length, mine = (lax.axis_size(axis), lax.axis_index(axis))
        pieces = gathered_once(
            jax.tree.map(
                lambda part, kind: part.astype(kind),
                so_far,
                (jnp.bfloat16, jnp.bfloat16, jnp.bfloat16, jnp.bfloat16),
            ),
            axis,
        )
        inside, so_far = (start, start)
        for k in range(length):
            passed = k < mine
            so_far = combine(
                so_far, jax.tree.map(lambda part, own: part[k].astype(own.dtype), pieces, shard)
            )
            inside = jax.tree.map(lambda new, old: jnp.where(passed, new, old), so_far, inside)
        before = combine(inside, before)
    return before


def in_blocks(shard, dim, length):
    before, after = (shard.shape[:dim], shard.shape[dim + 1 :])
    return jnp.moveaxis(shard.reshape(*before, length, -1, *after), dim, 0)


def sum_at_owner(shard, axis, dim):
    tiles = in_blocks(shard, dim, lax.axis_size(axis))
    arrived = lax.all_to_all(tiles, axis, split_axis=0, concat_axis=0, tiled=True)
    return arrived.astype(jnp.float32).sum(axis=0)


def rotate(values, places):
    half = values.shape[-1] // 2
    inverse = rope_base ** (-jnp.arange(half, dtype=jnp.float32) / half)
    angles = places[:, None] * inverse[None, :]
    cosine = jnp.cos(angles)[:, None, :]
    sine = jnp.sin(angles)[:, None, :]
    front = values[..., :half]
    back = values[..., half:]
    return jnp.concatenate([front * cosine - back * sine, back * cosine + front * sine], axis=-1)


def block_step(carried, inputs):
    query, keys, values, log_rate = inputs
    running = jnp.cumsum(log_rate, axis=0)
    spread = running[:, None, :] - running[None, :, :]
    length = log_rate.shape[0]
    lower = (jnp.arange(length)[:, None] >= jnp.arange(length)[None, :])[:, :, None]
    factor = jnp.where(lower, jnp.exp(jnp.minimum(spread, 0.0)), 0.0)
    scores = jnp.einsum("thd,shd->tsh", query, keys) * factor
    within = jnp.einsum("tsh,she->the", scores, values)
    across = jnp.einsum("thd,hde->the", query, carried) * jnp.exp(running)[:, :, None]
    tail_decay = jnp.exp(running[-1][None, :] - running)
    updated = jnp.exp(running[-1])[:, None, None] * carried + jnp.einsum(
        "shd,she->hde", keys * tail_decay[:, :, None], values
    )
    return (updated, within + across)


def head_norm(values):
    centre = values - jnp.mean(values, axis=-1, keepdims=True)
    spread = jnp.mean(centre * centre, axis=-1, keepdims=True)
    return centre * lax.rsqrt(spread + head_eps)


def local_group(query, keys, values, log_rate, width, places):
    length = query.shape[0]
    count_of_heads = query.shape[1] // width
    blocks = length // BLOCK

    def split(array):
        return array.astype(jnp.float32).reshape(length, count_of_heads, width)

    query_rot = rotate(split(query), places)
    keys_rot = rotate(split(keys), places) * width ** (-0.5)
    rates = log_rate.T
    carried = jnp.zeros((count_of_heads, width, width), jnp.float32)
    final_state, outputs = lax.scan(
        block_step,
        carried,
        (
            query_rot.reshape(blocks, BLOCK, count_of_heads, width),
            keys_rot.reshape(blocks, BLOCK, count_of_heads, width),
            split(values).reshape(blocks, BLOCK, count_of_heads, width),
            rates.reshape(blocks, BLOCK, count_of_heads),
        ),
    )
    running = jnp.cumsum(rates, axis=0)
    return (
        query_rot,
        outputs.reshape(length, count_of_heads, width),
        final_state,
        jnp.exp(running[-1]),
        running,
    )


def finish_group(query_rot, outputs, incoming, running, gate):
    length = outputs.shape[0]
    outputs = (
        outputs + jnp.einsum("thd,hde->the", query_rot, incoming) * jnp.exp(running)[:, :, None]
    )
    normed = head_norm(outputs).reshape(length, -1)
    return (jax.nn.silu(gate.astype(jnp.float32)) * normed).astype(jnp.bfloat16)


def chain(earlier, later):
    rate_wide, memory_wide, rate_narrow, memory_narrow = earlier
    later_rate_wide, later_memory_wide, later_rate_narrow, later_memory_narrow = later
    return (
        rate_wide * later_rate_wide,
        memory_wide * later_rate_wide[:, None, None] + later_memory_wide,
        rate_narrow * later_rate_narrow,
        memory_narrow * later_rate_narrow[:, None, None] + later_memory_narrow,
    )


def row_norm(middle, norm_gain):
    middle_f = middle.astype(jnp.float32)
    scale = lax.rsqrt(jnp.mean(middle_f * middle_f, axis=-1, keepdims=True) + norm_eps)
    return (middle_f * scale * norm_gain.astype(jnp.float32)).astype(jnp.bfloat16)


def on_device(
    stream_in,
    query_wide,
    key_wide,
    value_wide,
    gate_wide,
    decay_wide,
    query_narrow,
    key_narrow,
    value_narrow,
    gate_narrow,
    decay_narrow,
    output_wide,
    output_narrow,
    norm_gain,
    up_weight,
    down_weight,
):
    length = query_wide.shape[0]
    up_full, down_full = rows_first((up_weight, down_weight), SP, (0, 1))
    places = (lax.axis_index(SP) * length + jnp.arange(length, dtype=jnp.int32)).astype(jnp.float32)
    wide_query, wide_out, wide_state, wide_total, wide_running = local_group(
        query_wide, key_wide, value_wide, decay_wide, HDW, places
    )
    narrow_query, narrow_out, narrow_state, narrow_total, narrow_running = local_group(
        query_narrow, key_narrow, value_narrow, decay_narrow, HDN, places
    )
    identity = (
        jnp.ones_like(wide_total),
        jnp.zeros_like(wide_state),
        jnp.ones_like(narrow_total),
        jnp.zeros_like(narrow_state),
    )
    incoming = entering((wide_total, wide_state, narrow_total, narrow_state), SP, chain, identity)
    mixed_wide = finish_group(wide_query, wide_out, incoming[1], wide_running, gate_wide)
    mixed_narrow = finish_group(narrow_query, narrow_out, incoming[3], narrow_running, gate_narrow)
    mixed_sum = sum_at_owner(
        (
            jnp.dot(mixed_wide, output_wide, preferred_element_type=jnp.float32)
            + jnp.dot(mixed_narrow, output_narrow, preferred_element_type=jnp.float32)
        ).astype(jnp.bfloat16),
        "tp",
        0,
    )
    middle = (stream_in.astype(jnp.float32) + mixed_sum).astype(jnp.bfloat16)
    normed = lax.all_gather(row_norm(middle, norm_gain), "tp", axis=0, tiled=True)
    up_sum = jnp.dot(normed, up_full, preferred_element_type=jnp.float32)
    hidden = jnp.square(jax.nn.relu(up_sum)).astype(jnp.bfloat16)
    down_sum = jnp.dot(hidden, down_full, preferred_element_type=jnp.float32)
    down_rows = lax.psum_scatter(
        down_sum.astype(jnp.bfloat16), "tp", scatter_dimension=0, tiled=True
    ).astype(jnp.float32)
    return (middle.astype(jnp.float32) + down_rows).astype(jnp.bfloat16)


def solution(mesh):
    split = Mesh(mesh.devices.reshape(8, 4, 2, mesh.shape["tp"]), ("sp_0", "sp_1", "sp_2", "tp"))
    in_specs = (
        P(SP_TP, None),
        P(SP, "tp"),
        P(SP, "tp"),
        P(SP, "tp"),
        P(SP, "tp"),
        P("tp", SP),
        P(SP, "tp"),
        P(SP, "tp"),
        P(SP, "tp"),
        P(SP, "tp"),
        P("tp", SP),
        P("tp", None),
        P("tp", None),
        P(),
        P(SP, "tp"),
        P("tp", SP),
    )
    out_specs = P(SP_TP, None)
    return jax.shard_map(
        on_device, mesh=split, in_specs=in_specs, out_specs=out_specs, check_vma=False
    )
```

profile of v0, /device:TPU:1, one launch (start us, length us, event | category | flops | bytes accessed | tf_op | source)
XLA Modules:
  0.0 398.5 jit_solution(7533716243381743910)
XLA Ops:
  6.6 1.1 copy.156
  7.8 1.1 copy.158
  10.4 25.0 %while.27 = (s32[]{:T(128)}, f32[2,64,64]{2,1,0:T(8,128)S(1)}, f32[6,128,2,64]{1,0,3,2:T(8,128)}, f32[6,128,2]{2,1,0:T(8,128)S(1)}, f32[6,128,2,64]{1,0,3,2:T(8,...) while((s32[]{:T(128)}, f32[2,64,64]{2,1,0:T(8,128)S(1)}, ...), condition=%wide.region_5.6_spmd.clone, body=%wide.region_3.5_spmd.clone.sunk | while | flops 12877827 | bytes 1099440 | solution.py:132
  11.5 2.8 dynamic_update_slice.14
  15.7 2.8 dynamic_update_slice.14
  19.9 2.8 dynamic_update_slice.14
  24.0 2.8 dynamic_update_slice.14
  28.2 2.8 dynamic_update_slice.14
  32.3 2.8 dynamic_update_slice.14
  35.5 1.0 reshape_reshape.22
  36.5 1.9 fusion.88
  38.6 0.9 maximum_multiply_fusion.1
  39.5 22.9 %while.26 = (s32[]{:T(128)}, f32[1,128,128]{2,1,0:T(8,128)S(1)}, f32[6,128,1,128]{3,1,0,2:T(8,128)}, f32[6,128,1]{1,2,0:T(1,128)S(1)}, f32[6,128,1,128]{3,2,1,0:...) while((s32[]{:T(128)}, f32[1,128,128]{2,1,0:T(8,128)S(1)}, ...), condition=%wide.region_2.3_spmd.clone, body=%wide.region_0.2_spmd.clone.sunk | while | flops 17006596 | bytes 1515172 | solution.py:132
  67.1 4.7 %all-gather.3 = bf16[2,194,128]{2,1,0:T(8,128)(2,1)S(1)} all-gather(bf16[1,194,128]{2,1,0:T(8,128)(2,1)S(1)} %maximum_bitcast_fusion), channel_id=2, replica_groups=mesh['sp_0'=8,'sp_1'=4,'sp_2'=2,'tp'=4] {'sp_2'}, dimensions={0}, use_global_device_ids=true | all-gather | bytes 148992 | tf_op jit(solution)/shard_map/all_gather | solution.py:42
  74.8 9.3 %all-gather.4 = bf16[4,194,128]{2,1,0:T(8,128)(2,1)S(1)} all-gather(bf16[1,194,128]{2,1,0:T(8,128)(2,1)S(1)} %maximum_bitcast_fusion.1), channel_id=3, replica_groups=mesh['sp_0'=8,'sp_1'=4,'sp_2'=2,'tp'=4] {'sp_1'}, dimensions={0}, use_global_device_ids=true | all-gather | bytes 248320 | tf_op jit(solution)/shard_map/all_gather | solution.py:42
  89.2 21.5 %all-gather.5 = bf16[8,194,128]{2,1,0:T(8,128)(2,1)S(1)} all-gather(bf16[1,194,128]{2,1,0:T(8,128)(2,1)S(1)} %maximum_bitcast_fusion.2), channel_id=4, replica_groups=mesh['sp_0'=8,'sp_1'=4,'sp_2'=2,'tp'=4] {'sp_0'}, dimensions={0}, use_global_device_ids=true | all-gather | bytes 446976 | tf_op jit(solution)/shard_map/all_gather | solution.py:42
  113.8 0.7 copy.176
  114.5 0.7 copy.177
  115.3 0.7 copy.178
  116.1 0.7 copy.179
  116.9 0.7 copy.180
  117.6 0.8 reshape.1118
  118.4 0.7 copy.181
  119.1 0.8 reshape.1119
  119.9 0.7 copy.182
  120.6 0.8 reshape.1120
  121.5 0.7 copy.183
  122.2 0.8 reshape.1121
  123.0 0.7 copy.184
  123.8 0.7 copy.185
  124.6 0.7 copy.186
  125.4 1.6 fusion.292
  127.1 1.1 copy.170
  134.7 1.2 copy.169
  136.6 1.2 fusion.291
  137.8 1.1 copy.153
  139.1 1.0 fusion.93
  140.1 2.7 add_convert_fusion
  142.8 4.8 %all-to-all-start = ((bf16[4,192,2048]{2,1,0:T(8,128)(2,1)}), bf16[4,192,2048]{2,1,0:T(8,128)(2,1)}, u32[]{:S(2)}, u32[]{:S(2)}) async-start(bf16[4,192,2048]{2,1,0:T(8,128)(2,1)} %bitcast.454), calls=%async_computation | async-start | bytes 6291456 | tf_op jit(solution)/shard_map/all_to_all | solution.py:82
  147.8 27.9 %all-to-all-done = bf16[4,192,2048]{2,1,0:T(8,128)(2,1)} async-done(((bf16[4,192,2048]{2,1,0:T(8,128)(2,1)}), bf16[4,192,2048]{2,1,0:T(8,128)(2,1)}, u32[]{:S(2)}, u32[]{:S(2)}) %all-to-all-start) | async-done | bytes 3145760 | tf_op jit(solution)/shard_map/all_to_all | solution.py:82
  175.8 2.7 convert_reduce_fusion
  178.8 1.1 fusion.63
  180.1 0.7 pad_maximum_fusion.2
  180.9 47.7 %all-gather.9.cloned.1.call-done = bf16[768,2048]{1,0:T(8,128)(2,1)} async-done(((bf16[192,2048]{1,0:T(8,128)(2,1)}), bf16[768,2048]{1,0:T(8,128)(2,1)}) %all-gather.9.cloned.1.call-update) | async-done | bytes 3145744 | tf_op jit(solution)/shard_map/all_gather | solution.py:223
  228.6 102.9 %all-gather.11.cloned.1.call-done = bf16[2048,4096]{1,0:T(8,128)(2,1)} async-done(((bf16[32,4096]{1,0:T(8,128)(2,1)}), bf16[2048,4096]{1,0:T(8,128)(2,1)}) %all-gather.11.cloned.1.call-update) | async-done | bytes 16777232 | tf_op jit(solution)/shard_map/all_gather | solution.py:20
  331.5 20.7 %fusion.55 = bf16[768,2048]{1,0:T(8,128)(2,1)} fusion(bf16[2048,4096]{1,0:T(8,128)(2,1)} %all-gather.11.cloned.1.call-done, bf16[768,2048]{1,0:T(8,128)(2,1)} %all-gather.9.cloned.1.call-done), kind=kOutput, calls=%fused_computation.75 | convolution fusion | flops 12891193344 | bytes 23068672 | tf_op jit(solution)/shard_map/dot_general | solution.py:226
  352.2 37.5 %reduce-scatter.2.cloned.1.call-done = bf16[192,2048]{1,0:T(8,128)(2,1)} async-done(((bf16[768,2048]{1,0:T(8,128)(2,1)}), bf16[192,2048]{1,0:T(8,128)(2,1)}) %reduce-scatter.2.cloned.1.call-update) | async-done | bytes 786448 | tf_op jit(solution)/shard_map/reduce_scatter | solution.py:227
  389.7 2.3 fusion.64
  (304 shorter events, 39.7 us)
Async XLA Ops:
  6.5 132.5 %copy-start = (bf16[128,2048]{1,0:T(8,128)(2,1)S(1)}, bf16[128,2048]{1,0:T(8,128)(2,1)}, u32[]{:S(2)}) copy-start(bf16[128,2048]{1,0:T(8,128)(2,1)} %param.31) | copy-start | bytes 1572868
  6.5 3.0 copy-start.6
  7.8 2.3 copy-start.9
  10.4 26.1 %copy-start.4 = (bf16[768,128]{1,0:T(8,128)(2,1)S(1)}, bf16[768,128]{1,0:T(8,128)(2,1)}, u32[]{:S(2)}) copy-start(bf16[768,128]{1,0:T(8,128)(2,1)} %param.21) | copy-start | bytes 589828
  10.4 26.0 %copy-start.5 = (bf16[768,128]{1,0:T(8,128)(2,1)S(1)}, bf16[768,128]{1,0:T(8,128)(2,1)}, u32[]{:S(2)}) copy-start(bf16[768,128]{1,0:T(8,128)(2,1)} %param.22) | copy-start | bytes 589828
  36.5 3.0 copy-start.14
  71.8 15.4 %copy-start.15 = (f32[2]{0:T(128)}, f32[2]{0:T(128)S(1)}, u32[]{:S(2)}) copy-start(f32[2]{0:T(128)S(1)} %bitcast_convert_fusion.12) | copy-start | bytes 28
  73.3 52.0 %copy-start.3 = (f32[6,128,2,64]{1,0,3,2:T(8,128)S(1)}, f32[6,128,2,64]{1,0,3,2:T(8,128)}, u32[]{:S(2)}) copy-start(f32[6,128,2,64]{1,0,3,2:T(8,128)} %get-tuple-element.84) | copy-start | bytes 1179652
  87.2 0.9 copy-start.12
  87.2 1.1 copy-start.11
  87.2 23.5 %copy-start.10 = (f32[2]{0:T(128)}, f32[2]{0:T(128)S(1)}, u32[]{:S(2)}) copy-start(f32[2]{0:T(128)S(1)} %get-tuple-element.255) | copy-start | bytes 28
  139.0 1.1 copy-start.2
  142.8 5.0 %copy-start.13 = (bf16[2048]{0:T(1024)(128)(2,1)S(1)}, bf16[2048]{0:T(1024)(128)(2,1)}, u32[]{:S(2)}) copy-start(bf16[2048]{0:T(1024)(128)(2,1)} %param.33) | copy-start | bytes 12292
  142.8 33.0 %all-to-all-start = ((bf16[4,192,2048]{2,1,0:T(8,128)(2,1)}), bf16[4,192,2048]{2,1,0:T(8,128)(2,1)}, u32[]{:S(2)}, u32[]{:S(2)}) async-start(bf16[4,192,2048]{2,1,0:T(8,128)(2,1)} %bitcast.454), calls=%async_computation | async-start | bytes 6291456 | tf_op jit(solution)/shard_map/all_to_all | solution.py:82
  147.6 30.9 %copy-start.1 = (bf16[192,2048]{1,0:T(8,128)(2,1)S(1)}, bf16[192,2048]{1,0:T(8,128)(2,1)}, u32[]{:S(2)}) copy-start(bf16[192,2048]{1,0:T(8,128)(2,1)} %param.20) | copy-start | bytes 2359300
  147.6 81.0 %all-gather.9.cloned.1.call-start = ((), (), s32[]{:S(2)}) async-start(), calls=%async_computation.2 | async-start | bytes 3932160 | tf_op jit(solution)/shard_map/all_gather | solution.py:223
  178.5 1.6 copy-start.7
  178.5 1.6 copy-start.8
  180.0 151.5 %all-gather.11.cloned.1.call-start = ((), (), s32[]{:S(2)}) async-start(), calls=%async_computation.3 | async-start | bytes 17039360 | tf_op jit(solution)/shard_map/all_gather | solution.py:20
  180.8 208.9 %reduce-scatter.2.cloned.1.call-start = ((), (), s32[]{:S(2)}) async-start(), calls=%async_computation.4 | async-start | bytes 3932160 | tf_op jit(solution)/shard_map/reduce_scatter | solution.py:227
Sparse Core Ops, SparseCore 0:
  180.1 48.4 all-gather.8
  231.4 100.0 all-gather.10
  352.4 37.3 reduce-scatter.1
where the time goes:
time: 400 us; the launch traced here: 399 us
  waiting for transfers between devices  216 us (54%)
  local copies, waits for them, and re-layouts  50.2 us (13%)
  matrix products  35.7 us (9%)
  blocking collectives  35.5 us (9%)
  between operations  26.9 us (7%)
  other arithmetic  24.5 us (6%)
  starting transfers between devices  5.08 us (1%)
  loops' own time  4.6 us (1%)
    all_gather x1, waiting for transfers between devices, rows_first(): out, at, finished = (lax.all_gather(both, axis, axis=0, tiled=True), 0, [])  103 us
    all_gather x1, waiting for transfers between devices, on_device(): lax.all_gather(row_norm(middle, norm_gain), 'tp', axis=0, tiled=True)  47.7 us
    reduce_scatter x1, waiting for transfers between devices, on_device(): lax.psum_scatter(down_sum.astype(jnp.bfloat16), 'tp', scatter_dimension=0...  37.5 us
    all_gather x3, blocking collectives, gathered_once(): both, at, found = (lax.all_gather(jnp.concatenate(lines), axis), 0, {})  35.5 us
    all_to_all x1, waiting for transfers between devices, sum_at_owner(): lax.all_to_all(tiles, axis, split_axis=0, concat_axis=0, tiled=True)  27.9 us
    dynamic_update_slice x18, local copies, waits for them, and re-layouts, local_group(): lax.scan(block_step, carried, (query_rot.reshape(blocks, BLOCK, count_of_...  21.1 us
    dot_general x1, matrix products, on_device(): down_sum = jnp.dot(hidden, down_full, preferred_element_type=jnp.float32)  20.7 us
    convert_element_type x28, local copies, waits for them, and re-layouts, entering(): part[k].astype(own.dtype)  12.1 us
  transfers between devices with their start and end apart: 4, of which 4 were waited for; matrix products, arithmetic and copies ran while one was open for 0% of the time, Pallas kernels for 0%

commit v1 on v0

--- a/solution.py
+++ b/solution.py
@@ -220,7 +220,9 @@
         0,
     )
     middle = (stream_in.astype(jnp.float32) + mixed_sum).astype(jnp.bfloat16)
-    normed = lax.all_gather(row_norm(middle, norm_gain), "tp", axis=0, tiled=True)
+    shard_2 = row_norm(middle, norm_gain)
+    copies = jnp.concatenate([shard_2] * lax.axis_size("tp"), axis=0)
+    normed = lax.all_to_all(copies, "tp", 0, 0, tiled=True)
     up_sum = jnp.dot(normed, up_full, preferred_element_type=jnp.float32)
     hidden = jnp.square(jax.nn.relu(up_sum)).astype(jnp.bfloat16)
     down_sum = jnp.dot(hidden, down_full, preferred_element_type=jnp.float32)

time: 400 us -> 301 us (0.75)
  waiting for transfers between devices: 216 us -> 77.4 us
  blocking collectives: 35.5 us -> 73.5 us
    all_gather x1, waiting for transfers between devices: 103 us -> 0.01 us  [rows_first(): out, at, finished = (lax.all_gather(both, axis, axis=0, tiled=True), 0, [])]
    all_gather x1 -> x0, waiting for transfers between devices: 47.7 us -> none  [on_device(): lax.all_gather(row_norm(middle, norm_gain), 'tp', axis=0, tiled=True)]
    all_to_all x0 -> x1, blocking collectives: none -> 33 us  [on_device(): normed = lax.all_to_all(copies, 'tp', 0, 0, tiled=True)]
    reduce_scatter x1, waiting for transfers between devices: 37.5 us -> 46.7 us  [on_device(): lax.psum_scatter(down_sum.astype(jnp.bfloat16), 'tp', scatter_dimension=0...]
    all_gather x3, blocking collectives: 35.5 us -> 40.4 us  [gathered_once(): both, at, found = (lax.all_gather(jnp.concatenate(lines), axis), 0, {})]
  transfers between devices with their start and end apart: 4 -> 3, of which waited for: 4 -> 2; matrix products, arithmetic and copies ran while one was open for 0% -> 28% of each run, Pallas kernels for 0% -> 0%
where the time goes in v1:
time: 301 us; the launch traced here: 300 us
  waiting for transfers between devices  77.4 us (26%)
  blocking collectives  73.5 us (24%)
  local copies, waits for them, and re-layouts  52.8 us (18%)
  matrix products  36 us (12%)
  between operations  26.9 us (9%)
  other arithmetic  23.4 us (8%)
  starting transfers between devices  5.01 us (2%)
  loops' own time  4.82 us (2%)
    reduce_scatter x1, waiting for transfers between devices, on_device(): lax.psum_scatter(down_sum.astype(jnp.bfloat16), 'tp', scatter_dimension=0...  46.7 us
    all_gather x3, blocking collectives, gathered_once(): both, at, found = (lax.all_gather(jnp.concatenate(lines), axis), 0, {})  40.4 us
    all_to_all x1, blocking collectives, on_device(): normed = lax.all_to_all(copies, 'tp', 0, 0, tiled=True)  33 us
    all_to_all x1, waiting for transfers between devices, sum_at_owner(): lax.all_to_all(tiles, axis, split_axis=0, concat_axis=0, tiled=True)  30.6 us
    dynamic_update_slice x18, local copies, waits for them, and re-layouts, local_group(): lax.scan(block_step, carried, (query_rot.reshape(blocks, BLOCK, count_of_...  21.1 us
    dot_general x1, matrix products, on_device(): down_sum = jnp.dot(hidden, down_full, preferred_element_type=jnp.float32)  20.7 us
    convert_element_type x28, local copies, waits for them, and re-layouts, entering(): part[k].astype(own.dtype)  11 us
  transfers between devices with their start and end apart: 3, of which 2 were waited for; matrix products, arithmetic and copies ran while one was open for 28% of the time, Pallas kernels for 0%

profile of v1, /device:TPU:1, one launch (start us, length us, event | category | flops | bytes accessed | tf_op | source)
XLA Modules:
  0.0 299.9 jit_solution(14953674954953249489)
XLA Ops:
  6.5 1.7 pad_maximum_fusion.3
  8.4 1.1 copy.156
  9.5 1.1 copy.158
  12.2 25.0 %while.27 = (s32[]{:T(128)}, f32[2,64,64]{2,1,0:T(8,128)S(1)}, f32[6,128,2,64]{1,0,3,2:T(8,128)}, f32[6,128,2]{2,1,0:T(8,128)S(1)}, f32[6,128,2,64]{1,0,3,2:T(8,...) while((s32[]{:T(128)}, f32[2,64,64]{2,1,0:T(8,128)S(1)}, ...), condition=%wide.region_5.6_spmd.clone, body=%wide.region_3.5_spmd.clone.sunk | while | flops 12877827 | bytes 1099440 | solution.py:132
  13.3 2.8 dynamic_update_slice.14
  17.4 2.8 dynamic_update_slice.14
  21.6 2.8 dynamic_update_slice.14
  25.8 2.8 dynamic_update_slice.14
  29.9 2.8 dynamic_update_slice.14
  34.1 2.8 dynamic_update_slice.14
  37.2 1.0 reshape_reshape.22
  43.3 1.9 fusion.88
  45.4 0.9 maximum_multiply_fusion.1
  46.3 23.6 %while.26 = (s32[]{:T(128)}, f32[1,128,128]{2,1,0:T(8,128)S(1)}, f32[6,128,1,128]{3,1,0,2:T(8,128)}, f32[6,128,1]{1,2,0:T(1,128)S(1)}, f32[6,128,1,128]{3,2,1,0:...) while((s32[]{:T(128)}, f32[1,128,128]{2,1,0:T(8,128)S(1)}, ...), condition=%wide.region_2.3_spmd.clone, body=%wide.region_0.2_spmd.clone.sunk | while | flops 17006596 | bytes 1515172 | solution.py:132
  48.8 0.6 constant_dynamic-update-slice_fusion.2
  52.7 0.6 constant_dynamic-update-slice_fusion.2
  70.0 4.8 %all-gather.3 = bf16[2,194,128]{2,1,0:T(8,128)(2,1)S(1)} all-gather(bf16[1,194,128]{2,1,0:T(8,128)(2,1)S(1)} %maximum_bitcast_fusion), channel_id=2, replica_groups=mesh['sp_0'=8,'sp_1'=4,'sp_2'=2,'tp'=4] {'sp_2'}, dimensions={0}, use_global_device_ids=true | all-gather | bytes 148992 | tf_op jit(solution)/shard_map/all_gather | solution.py:42
  78.8 11.7 %all-gather.4 = bf16[4,194,128]{2,1,0:T(8,128)(2,1)S(1)} all-gather(bf16[1,194,128]{2,1,0:T(8,128)(2,1)S(1)} %maximum_bitcast_fusion.1), channel_id=3, replica_groups=mesh['sp_0'=8,'sp_1'=4,'sp_2'=2,'tp'=4] {'sp_1'}, dimensions={0}, use_global_device_ids=true | all-gather | bytes 248320 | tf_op jit(solution)/shard_map/all_gather | solution.py:42
  96.6 24.0 %all-gather.5 = bf16[8,194,128]{2,1,0:T(8,128)(2,1)S(1)} all-gather(bf16[1,194,128]{2,1,0:T(8,128)(2,1)S(1)} %maximum_bitcast_fusion.2), channel_id=4, replica_groups=mesh['sp_0'=8,'sp_1'=4,'sp_2'=2,'tp'=4] {'sp_0'}, dimensions={0}, use_global_device_ids=true | all-gather | bytes 446976 | tf_op jit(solution)/shard_map/all_gather | solution.py:42
  120.7 0.7 copy.173
  121.5 0.7 copy.174
  122.3 0.7 copy.175
  123.0 0.7 copy.176
  123.8 0.7 copy.177
  124.6 0.7 copy.178
  125.4 0.7 copy.179
  126.2 0.7 copy.180
  127.0 0.7 copy.181
  127.8 0.7 copy.182
  128.6 0.7 copy.183
  129.4 0.7 copy.184
  130.2 0.7 copy.185
  131.0 0.7 copy.186
  131.8 1.1 copy.170
  139.4 1.9 copy.169
  141.3 1.1 copy.153
  143.0 0.7 fusion.269
  143.7 1.5 fusion.291
  145.3 1.5 fusion.292
  147.2 1.0 fusion.93
  148.2 2.7 add_convert_fusion
  150.9 4.8 %all-to-all-start = ((bf16[4,192,2048]{2,1,0:T(8,128)(2,1)}), bf16[4,192,2048]{2,1,0:T(8,128)(2,1)}, u32[]{:S(2)}, u32[]{:S(2)}) async-start(bf16[4,192,2048]{2,1,0:T(8,128)(2,1)} %bitcast.456), calls=%async_computation | async-start | bytes 6291456 | tf_op jit(solution)/shard_map/all_to_all | solution.py:82
  156.0 30.6 %all-to-all-done = bf16[4,192,2048]{2,1,0:T(8,128)(2,1)} async-done(((bf16[4,192,2048]{2,1,0:T(8,128)(2,1)}), bf16[4,192,2048]{2,1,0:T(8,128)(2,1)}, u32[]{:S(2)}, u32[]{:S(2)}) %all-to-all-start) | async-done | bytes 3145760 | tf_op jit(solution)/shard_map/all_to_all | solution.py:82
  186.6 2.6 convert_reduce_fusion
  190.3 33.0 %all_to_all.17 = bf16[4,192,2048]{2,1,0:T(8,128)(2,1)} all-to-all(bf16[4,192,2048]{2,1,0:T(8,128)(2,1)S(1)} %bitcast.457), channel_id=1, replica_groups=mesh['sp_0'=8,'sp_1'=4,'sp_2'=2,'tp'=4] {'tp'}, dimensions={0} | all-to-all | bytes 6291456 | tf_op jit(solution)/shard_map/all_to_all | solution.py:225
  223.3 20.7 %fusion.55 = bf16[768,2048]{1,0:T(8,128)(2,1)} fusion(bf16[2048,4096]{1,0:T(8,128)(2,1)} %all-gather.8.cloned.1.call-done, bf16[768,2048]{1,0:T(8,128)(2,1)} %bitcast.465), kind=kOutput, calls=%fused_computation.75 | convolution fusion | flops 12891193344 | bytes 23068672 | tf_op jit(solution)/shard_map/dot_general | solution.py:228
  244.1 46.7 %reduce-scatter.2.cloned.1.call-done = bf16[192,2048]{1,0:T(8,128)(2,1)} async-done(((bf16[768,2048]{1,0:T(8,128)(2,1)}), bf16[192,2048]{1,0:T(8,128)(2,1)}) %reduce-scatter.2.cloned.1.call-update) | async-done | bytes 786448 | tf_op jit(solution)/shard_map/reduce_scatter | solution.py:229
  290.8 2.2 fusion.64
  (315 shorter events, 39.8 us)
Async XLA Ops:
  6.5 140.6 %copy-start = (bf16[128,2048]{1,0:T(8,128)(2,1)S(1)}, bf16[128,2048]{1,0:T(8,128)(2,1)}, u32[]{:S(2)}) copy-start(bf16[128,2048]{1,0:T(8,128)(2,1)} %param.31) | copy-start | bytes 1572868
  6.5 216.8 %all-gather.8.cloned.1.call-start = ((), (), s32[]{:S(2)}) async-start(), calls=%async_computation.3 | async-start | bytes 17039360 | tf_op jit(solution)/shard_map/all_gather | solution.py:20
  8.3 3.0 copy-start.11
  9.5 2.4 copy-start.12
  12.1 26.1 %copy-start.19 = (f32[1,768]{1,0:T(1,128)S(1)}, f32[1,768]{1,0:T(1,128)}, u32[]{:S(2)}) copy-start(f32[1,768]{1,0:T(1,128)} %param.25) | copy-start | bytes 9220
  12.1 31.1 %copy-start.9 = (bf16[768,128]{1,0:T(8,128)(2,1)S(1)}, bf16[768,128]{1,0:T(8,128)(2,1)}, u32[]{:S(2)}) copy-start(bf16[768,128]{1,0:T(8,128)(2,1)} %param.21) | copy-start | bytes 589828
  12.1 31.1 %copy-start.10 = (bf16[768,128]{1,0:T(8,128)(2,1)S(1)}, bf16[768,128]{1,0:T(8,128)(2,1)}, u32[]{:S(2)}) copy-start(bf16[768,128]{1,0:T(8,128)(2,1)} %param.22) | copy-start | bytes 589828
  38.9 0.5 copy-start.21
  75.9 0.6 copy-start.14
  76.7 0.5 copy-start.20
  77.3 54.4 %copy-start.3 = (f32[6,128,2,64]{1,0,3,2:T(8,128)S(1)}, f32[6,128,2,64]{1,0,3,2:T(8,128)}, u32[]{:S(2)}) copy-start(f32[6,128,2,64]{1,0,3,2:T(8,128)} %get-tuple-element.84) | copy-start | bytes 1179652
  94.0 0.5 copy-start.13
  94.7 0.6 copy-start.15
  94.7 0.7 copy-start.17
  94.7 0.9 copy-start.16
  131.8 13.5 %copy-start.4 = (f32[2,64,64]{1,2,0:T(8,128)S(1)}, f32[2,64,64]{1,2,0:T(8,128)}, u32[]{:S(2)}) copy-start(f32[2,64,64]{1,2,0:T(8,128)} %copy.181) | copy-start | bytes 98308
  131.8 13.5 %copy-start.5 = (f32[2,64,64]{1,2,0:T(8,128)S(1)}, f32[2,64,64]{1,2,0:T(8,128)}, u32[]{:S(2)}) copy-start(f32[2,64,64]{1,2,0:T(8,128)} %copy.182) | copy-start | bytes 98308
  131.8 13.5 %copy-start.6 = (f32[2,64,64]{1,2,0:T(8,128)S(1)}, f32[2,64,64]{1,2,0:T(8,128)}, u32[]{:S(2)}) copy-start(f32[2,64,64]{1,2,0:T(8,128)} %copy.183) | copy-start | bytes 98308
  131.8 13.5 %copy-start.7 = (f32[2,64,64]{1,2,0:T(8,128)S(1)}, f32[2,64,64]{1,2,0:T(8,128)}, u32[]{:S(2)}) copy-start(f32[2,64,64]{1,2,0:T(8,128)} %copy.184) | copy-start | bytes 98308
  131.8 13.5 %copy-start.8 = (f32[2,64,64]{1,2,0:T(8,128)S(1)}, f32[2,64,64]{1,2,0:T(8,128)}, u32[]{:S(2)}) copy-start(f32[2,64,64]{1,2,0:T(8,128)} %copy.185) | copy-start | bytes 98308
  147.2 1.1 copy-start.2
  150.9 5.0 %copy-start.18 = (bf16[2048]{0:T(1024)(128)(2,1)S(1)}, bf16[2048]{0:T(1024)(128)(2,1)}, u32[]{:S(2)}) copy-start(bf16[2048]{0:T(1024)(128)(2,1)} %param.33) | copy-start | bytes 12292
  150.9 35.7 %all-to-all-start = ((bf16[4,192,2048]{2,1,0:T(8,128)(2,1)}), bf16[4,192,2048]{2,1,0:T(8,128)(2,1)}, u32[]{:S(2)}, u32[]{:S(2)}) async-start(bf16[4,192,2048]{2,1,0:T(8,128)(2,1)} %bitcast.456), calls=%async_computation | async-start | bytes 6291456 | tf_op jit(solution)/shard_map/all_to_all | solution.py:82
  155.7 33.5 %copy-start.1 = (bf16[192,2048]{1,0:T(8,128)(2,1)S(1)}, bf16[192,2048]{1,0:T(8,128)(2,1)}, u32[]{:S(2)}) copy-start(bf16[192,2048]{1,0:T(8,128)(2,1)} %param.20) | copy-start | bytes 2359300
  155.7 135.1 %reduce-scatter.2.cloned.1.call-start = ((), (), s32[]{:S(2)}) async-start(), calls=%async_computation.4 | async-start | bytes 3932160 | tf_op jit(solution)/shard_map/reduce_scatter | solution.py:229
Sparse Core Ops, SparseCore 0:
  10.1 107.1 all-gather.7
  244.2 46.5 reduce-scatter.1
